TPU v7x, 1024 devices: a whole 4x8x16 slice. The times are simulated.
1024 devices in a mesh: sp: 16 (over z), dp: 64 (over y, x, core).
Axes of the slice: x: 4, y: 8, z: 16, core: 2. Of those that a mesh axis runs over, the one named last changes fastest.
Arguments:
- hidden: bfloat16 [64, 2048, 2048], P('dp', 'sp'), may hold values from -6 to 6
- queries: bfloat16 [64, 2048, 1024], P('dp', 'sp'), may hold values from -6 to 6
- values: bfloat16 [64, 2048, 2048], P('dp', 'sp'), may hold values from -6 to 6
- key_weight: bfloat16 [2048, 1024], P('dp'), may hold values from -0.125 to 0.125
- decay_down: bfloat16 [2048, 16], replicated, may hold values from -0.125 to 0.125
- decay_up: float32 [16, 1024], replicated, may hold values from -1.5 to 1.5
- decay_bias: float32 [1024], replicated, may hold values from -1 to 8
- span_shift: bfloat16 [64, 2048], P('dp', 'sp'), may hold values from -1.5 to 1.5, as said below
- norm_gain: float32 [2048], replicated, may hold values from 0.1 to 1.9
Outputs:
- attended: bfloat16 [64, 2048, 2048], P('dp', 'sp')
Inputs may be any that keep to these rules, and one draw needn't show every extreme that they name: `span_shift`: constant over each aligned block of 64 positions.
All inputs are finite; a program needn't handle non-finite values.
Results may differ from a plain program's by a relative error of at most 0.0073.
Values may be sent and summed in bfloat16 or wider, within the bound.
A program may use at most 64 MiB of HBM per device.

v0:
```python
import jax
import jax.numpy as jnp
from jax import lax
from jax.sharding import Mesh
from jax.sharding import PartitionSpec as P

HEADS = 4
DK = 256
DV = 512
BLOCK = 64
KEY = 1024
VAL = 2048
DP = ("dp_0", "dp_1", "dp_2")


decay_tau = 16.0
norm_eps = 1e-05
highest = lax.Precision.HIGHEST


def in_order(parts, dim):
    parts = jnp.moveaxis(parts, 0, dim)
    shape = parts.shape
    return parts.reshape(*shape[:dim], shape[dim] * shape[dim + 1], *shape[dim + 2 :])


def gather_in_order(shard, axes, sequence):
    parts = shard
    for k in sequence:
        parts = lax.all_gather(parts, axes[k])
    done = sequence[::-1]
    back = [done.index(k) for k in range(len(axes))]
    parts = parts.transpose(*back, *range(len(axes), parts.ndim))
    return parts.reshape(-1, *shard.shape)


def gathered_by_axis(shard, axes, sequence, dim):
    return in_order(gather_in_order(shard, axes, sequence), dim)


def side_by_side(arrays, axis, split_dim, concat_dim, along):
    ends, at = ([], 0)
    for a in arrays[:-1]:
        at += a.shape[along]
        ends.append(at)
    both = jnp.concatenate(arrays, axis=along)
    return tuple(
        jnp.split(
            lax.all_to_all(both, axis, split_axis=split_dim, concat_axis=concat_dim, tiled=True),
            ends,
            axis=along,
        )
    )


def in_blocks(shard, dim, peers):
    shape = shard.shape
    parts = shard.reshape(*shape[:dim], peers, shape[dim] // peers, *shape[dim + 1 :])
    return jnp.moveaxis(parts, dim, 0)


def cut_rows(length, count):
    unit = 8 if length >= 8 * count else 1
    return [length // unit * k // count * unit for k in range(1, count)]


def exchange_in_pieces(shard, axis, pieces, split_dim, concat_dim):
    parts = in_blocks(shard, split_dim, lax.axis_size(axis))
    split_at = max(range(1, max(2, parts.ndim - 1)), key=lambda d: parts.shape[d])
    outs = []
    for piece in jnp.split(parts, cut_rows(parts.shape[split_at], pieces), axis=split_at):
        if piece.size:
            outs.append(lax.all_to_all(piece, axis, split_axis=0, concat_axis=0, tiled=True))
    return in_order(jnp.concatenate(outs, axis=split_at), concat_dim)


def mechanism(query, keys_in, value_in, log_decay):
    length, key_width = query.shape
    value_width = value_in.shape[-1]
    blocks = length // BLOCK
    step_decay = log_decay.reshape(blocks, BLOCK, key_width)
    inclusive = jnp.cumsum(step_decay, axis=1)
    exclusive = inclusive - step_decay
    total = inclusive[:, -1, :]
    query3 = query.reshape(blocks, BLOCK, key_width)
    keys3 = keys_in.reshape(blocks, BLOCK, key_width)
    value_tensor3 = value_in.reshape(blocks, BLOCK, value_width)
    query_forward_part = (query3 * jnp.exp(inclusive)).astype(jnp.bfloat16)
    key_fwd = (keys3 * jnp.exp(-inclusive)).astype(jnp.bfloat16)
    query_reverse_part = (query3 * jnp.exp(-exclusive)).astype(jnp.bfloat16)
    key_bwd = (keys3 * jnp.exp(exclusive)).astype(jnp.bfloat16)
    key_end = (keys3 * jnp.exp(total[:, None, :] - inclusive)).astype(jnp.bfloat16)
    fwd_scores = jnp.einsum(
        "nid,njd->nij", query_forward_part, key_fwd, preferred_element_type=jnp.float32
    )
    bwd_scores = jnp.einsum(
        "nid,njd->nij", query_reverse_part, key_bwd, preferred_element_type=jnp.float32
    )
    row_index = lax.broadcasted_iota(jnp.int32, (BLOCK, BLOCK), 0)
    col_index = lax.broadcasted_iota(jnp.int32, (BLOCK, BLOCK), 1)
    attention_scores = jnp.where((col_index <= row_index)[None], fwd_scores, bwd_scores).astype(
        jnp.bfloat16
    )
    inner_block_term = jnp.einsum(
        "ucy,uyh->uch", attention_scores, value_tensor3, preferred_element_type=jnp.float32
    )
    end_terms = jnp.einsum(
        "njd,nje->nde", key_end, value_tensor3, preferred_element_type=jnp.float32
    )
    start_terms = jnp.einsum(
        "njd,nje->nde", key_bwd, value_tensor3, preferred_element_type=jnp.float32
    )
    rates = jnp.exp(total)

    def forward_step(carry_state, inputs):
        rate, term = inputs
        return (rate[:, None] * carry_state + term, carry_state)

    def backward_step(carry_state, inputs):
        rate, term = inputs
        state_here = rate[:, None] * carry_state
        return (state_here + term, state_here)

    empty = jnp.zeros((key_width, value_width), jnp.float32)
    _, forward_scan_states = lax.scan(forward_step, empty, (rates, end_terms))
    _, reverse_scan_states = lax.scan(backward_step, empty, (rates, start_terms), reverse=True)
    produced_rows = jnp.einsum(
        "tzv,tvg->tzg",
        query_forward_part,
        forward_scan_states.astype(jnp.bfloat16),
        preferred_element_type=jnp.float32,
    )
    produced_rows = produced_rows + jnp.einsum(
        "tzv,tvg->tzg",
        query_reverse_part,
        reverse_scan_states.astype(jnp.bfloat16),
        preferred_element_type=jnp.float32,
    )
    return (inner_block_term + produced_rows).reshape(length, value_width).astype(jnp.bfloat16)


def body(
    hidden, queries, values, key_weight, decay_down, decay_up, decay_bias, span_shift, norm_gain
):
    seq_count, tok_count, model_width = hidden.shape
    group_size = lax.axis_size("sp")
    value_split = group_size // HEADS
    part_width = DV // value_split
    head_index = lax.axis_index("sp") // value_split
    token_rows = hidden.reshape(tok_count, model_width)

    def per_item(tensor, width):
        by_head = tensor.reshape(tok_count, HEADS, width).transpose(1, 0, 2)
        spread_out = jnp.broadcast_to(by_head[:, None], (HEADS, value_split, tok_count, width))
        return spread_out.reshape(group_size, tok_count, width)

    def every_item(tensor):
        return jnp.broadcast_to(tensor[None], (group_size,) + tensor.shape)

    key_sums = jnp.dot(
        token_rows,
        gathered_by_axis(key_weight, DP, (1, 0, 2), 0),
        preferred_element_type=jnp.float32,
    )
    keys = key_sums.astype(jnp.bfloat16)
    head_key = lax.all_to_all(per_item(keys, DK), "sp", split_axis=0, concat_axis=1, tiled=True)[0]
    low = jnp.dot(token_rows, decay_down, preferred_element_type=jnp.float32).astype(jnp.bfloat16)
    value_items = values.reshape(tok_count, group_size, part_width).transpose(1, 0, 2)
    head_query, head_value, head_low, head_shift = side_by_side(
        (
            per_item(queries.reshape(tok_count, KEY), DK),
            value_items,
            every_item(low),
            every_item(span_shift.reshape(tok_count, 1)),
        ),
        "sp",
        0,
        1,
        2,
    )
    up_columns = lax.dynamic_slice_in_dim(decay_up, head_index * DK, DK, 1)
    bias_part = lax.dynamic_slice_in_dim(decay_bias, head_index * DK, DK, 0)
    pre = jnp.dot(
        head_low[0].astype(jnp.float32),
        up_columns,
        precision=highest,
        preferred_element_type=jnp.float32,
    )
    pre = pre + bias_part[None, :] + head_shift[0].astype(jnp.float32)
    log_decay = jax.nn.log_sigmoid(pre) / decay_tau
    scaled = head_query[0].astype(jnp.float32) * DK ** (-0.5)
    mixed = mechanism(scaled, head_key.astype(jnp.float32), head_value[0], log_decay)
    returned = exchange_in_pieces(mixed[None], "sp", 2, 1, 0)
    grouped = returned.astype(jnp.float32).transpose(1, 0, 2).reshape(tok_count, HEADS, DV)
    normed = grouped * lax.rsqrt(jnp.mean(grouped * grouped, axis=-1, keepdims=True) + norm_eps)
    normed = normed * norm_gain.reshape(HEADS, DV)[None]
    return normed.reshape(seq_count, tok_count, VAL).astype(jnp.bfloat16)


def solution(mesh):
    split = Mesh(mesh.devices.reshape(mesh.shape["sp"], 8, 4, 2), ("sp", "dp_0", "dp_1", "dp_2"))
    placed = (
        P(DP, "sp", None),
        P(DP, "sp", None),
        P(DP, "sp", None),
        P(DP, None),
        P(),
        P(),
        P(),
        P(DP, "sp"),
        P(),
    )
    return jax.shard_map(
        body, mesh=split, in_specs=placed, out_specs=P(DP, "sp", None), check_vma=False
    )
```

profile of v0, /device:TPU:56, one launch (start us, length us, event | category | flops | bytes accessed | tf_op | source)
XLA Modules:
  0.0 361.4 jit_solution(4902827169057596006)
XLA Ops:
  6.5 14.3 %all-gather = bf16[128,1024]{1,0:T(8,128)(2,1)} all-gather(bf16[32,1024]{1,0:T(8,128)(2,1)} %param.16), channel_id=2, replica_groups=mesh['sp'=16,'dp_0'=8,'dp_1'=4,'dp_2'=2] {'dp_1'}, dimensions={0}, use_global_device_ids=true | all-gather | bytes 327680 | tf_op jit(solution)/shard_map/all_gather | solution.py:30
  20.9 1.3 copy.78
  22.2 1.1 reshape_reshape.6
  24.1 1.3 pad_maximum_fusion
  25.4 18.9 %all-to-all-start = ((bf16[16,128,401]{1,2,0:T(8,128)(2,1)}), bf16[16,128,401]{1,2,0:T(8,128)(2,1)S(1)}, u32[]{:S(2)}, u32[]{:S(2)}) async-start(bf16[16,128,401]{1,2,0:T(8,128)(2,1)} %pad_maximum_fusion), calls=%async_computation | async-start | bytes 3342336 | tf_op jit(solution)/shard_map/all_to_all | solution.py:49
  44.4 30.5 %all-gather.6.cloned.1.call-done = bf16[32,32,1024]{2,1,0:T(8,128)(2,1)} async-done(((bf16[4,32,1024]{2,1,0:T(8,128)(2,1)}), bf16[32,32,1024]{2,1,0:T(8,128)(2,1)}) %all-gather.6.cloned.1.call-update) | async-done | bytes 2097168 | tf_op jit(solution)/shard_map/all_gather | solution.py:30
  74.9 29.5 %all-gather.8.cloned.1.call-done = bf16[16,4,32,1024]{3,2,1,0:T(8,128)(2,1)} async-done(((bf16[8,4,32,1024]{3,2,1,0:T(8,128)(2,1)}), bf16[16,4,32,1024]{3,2,1,0:T(8,128)(2,1)}) %all-gather.8.cloned.1.call-update) | async-done | bytes 4194320 | tf_op jit(solution)/shard_map/all_gather | solution.py:30
  104.4 2.6 copy.82
  108.0 8.0 %all-to-all-done = bf16[16,128,401]{1,2,0:T(8,128)(2,1)S(1)} async-done(((bf16[16,128,401]{1,2,0:T(8,128)(2,1)}), bf16[16,128,401]{1,2,0:T(8,128)(2,1)S(1)}, u32[]{:S(2)}, u32[]{:S(2)}) %all-to-all-start) | async-done | bytes 1642528 | tf_op jit(solution)/shard_map/all_to_all | solution.py:49
  116.0 1.3 broadcast_in_dim.59
  117.3 10.3 %all-to-all-start.1 = ((bf16[16,128,256]{2,1,0:T(8,128)(2,1)}), bf16[16,128,256]{2,1,0:T(8,128)(2,1)}, u32[]{:S(2)}, u32[]{:S(2)}) async-start(bf16[16,128,256]{2,1,0:T(8,128)(2,1)} %bitcast.16), calls=%async_computation.1 | async-start | bytes 2097152 | tf_op jit(solution)/shard_map/all_to_all | solution.py:166
  128.4 2.8 copy.79
  131.8 2.8 fusion.3
  134.6 1.3 fusion.8
  136.9 1.5 convert_multiply_fusion
  138.4 39.4 %all-to-all-done.1 = bf16[16,128,256]{2,1,0:T(8,128)(2,1)} async-done(((bf16[16,128,256]{2,1,0:T(8,128)(2,1)}), bf16[16,128,256]{2,1,0:T(8,128)(2,1)}, u32[]{:S(2)}, u32[]{:S(2)}) %all-to-all-start.1) | async-done | bytes 1048608 | tf_op jit(solution)/shard_map/all_to_all | solution.py:166
  177.7 1.6 convert.4
  179.6 6.9 %multiply_convert_fusion = (bf16[32,64,256]{2,0,1:T(8,128)(2,1)}, bf16[32,64,256]{2,0,1:T(8,128)(2,1)S(1)}, bf16[32,64,256]{2,0,1:T(8,128)(2,1)}, bf16[32,64,256]{2,0,1:T(8,128)(2,1)}, bf16[32,64,256]{2,0,1:T(8,128)(2,1)}) fusion(f32[32,64,256]{2,0,1:T(8,128)S(1)} %fusion.8, f32[32,64,256]{2,1,0:T(8,128)S(1)} %convert.4, ...), kind=kLoop, calls=%fused_computation.17 | loop fusion | flops 7340032 | bytes 13664256 | tf_op jit(solution)/shard_map/convert_element_type | solution.py:92
  186.5 2.9 fusion.28
  189.9 38.1 %while.31 = (s32[]{:T(128)}, f32[256,128]{1,0:T(8,128)S(1)}, bf16[32,256,128]{2,1,0:T(8,128)(2,1)S(1)}, f32[32,256]{1,0:T(8,128)S(1)}, f32[32,256,128]{2,1,0:T(8,128)}, /*index=5*/s32[]{:T(128)}, s32[]{:T(128)}, s32[]{:T(128)}) while((s32[]{:T(128)}, f32[256,128]{1,0:T(8,128)S(1)}, bf16[32,256,128]{2,1,0:T(8,128)(2,1)S(1)}, ...), condition=%wide.region_4.5_spmd.clone, body=%wide.region_3.4_spmd.clone.sunk | while | flops 163844 | bytes 659584 | solution.py:126
  190.1 1.0 bitcast_add_fusion.5
  191.3 1.0 bitcast_add_fusion.5
  192.5 1.0 bitcast_add_fusion.5
  193.7 1.0 bitcast_add_fusion.5
  194.9 1.0 bitcast_add_fusion.5
  196.1 1.0 bitcast_add_fusion.5
  197.3 1.0 bitcast_add_fusion.5
  198.5 1.0 bitcast_add_fusion.5
  199.6 1.0 bitcast_add_fusion.5
  200.8 1.0 bitcast_add_fusion.5
  202.0 1.0 bitcast_add_fusion.5
  203.2 1.0 bitcast_add_fusion.5
  204.4 1.0 bitcast_add_fusion.5
  205.6 1.0 bitcast_add_fusion.5
  206.8 1.0 bitcast_add_fusion.5
  208.0 1.0 bitcast_add_fusion.5
  209.2 1.0 bitcast_add_fusion.5
  210.4 1.0 bitcast_add_fusion.5
  211.6 1.0 bitcast_add_fusion.5
  212.7 1.0 bitcast_add_fusion.5
  213.9 1.0 bitcast_add_fusion.5
  215.1 1.0 bitcast_add_fusion.5
  216.3 1.0 bitcast_add_fusion.5
  217.5 1.0 bitcast_add_fusion.5
  218.7 1.0 bitcast_add_fusion.5
  219.9 1.0 bitcast_add_fusion.5
  221.1 1.0 bitcast_add_fusion.5
  222.3 1.0 bitcast_add_fusion.5
  223.5 1.0 bitcast_add_fusion.5
  224.7 1.0 bitcast_add_fusion.5
  225.9 1.0 bitcast_add_fusion.5
  227.0 1.0 bitcast_add_fusion.5
  228.1 4.2 %fusion.24 = f32[32,256,128]{2,1,0:T(8,128)} fusion(bf16[32,64,128]{2,1,0:T(8,128)(2,1)S(1)} %bitcast.96, bf16[32,64,256]{2,0,1:T(8,128)(2,1)} %get-tuple-element.193), kind=kOutput, calls=%fused_computation.40 | convolution fusion | flops 134217728 | bytes 5767168 | tf_op jit(solution)/shard_map/njd,nje->nde/dot_general | solution.py:107
  232.2 1.8 broadcast.49.clone.1
  234.1 54.3 %while.30 = (s32[]{:T(128)}, f32[256,128]{1,0:T(8,128)S(1)}, bf16[32,256,128]{2,1,0:T(8,128)(2,1)}, f32[32,256]{1,0:T(8,128)S(1)}, f32[32,256,128]{2,1,0:T(8,128)}, /*index=5*/s32[]{:T(128)}, s32[]{:T(128)}) while((s32[]{:T(128)}, f32[256,128]{1,0:T(8,128)S(1)}, bf16[32,256,128]{2,1,0:T(8,128)(2,1)}, f32[32,256]{1,0:T(8,128)S(1)}, ...), condition=%wide.region_2.3_spmd.clone, body=%wide.region_1.2_spmd.clone.sunk | while | flops 131075 | bytes 593004 | solution.py:125
  239.8 1.0 bitcast_add_fusion.4
  243.2 1.0 bitcast_add_fusion.4
  288.3 3.7 %fusion.26 = bf16[32,64,64]{2,1,0:T(8,128)(2,1)} fusion(bf16[32,64,256]{2,0,1:T(8,128)(2,1)} %get-tuple-element.197, bf16[32,64,256]{2,0,1:T(8,128)(2,1)} %get-tuple-element.196), kind=kOutput, calls=%fused_computation.42 | convolution fusion | flops 67108864 | bytes 2359296 | tf_op jit(solution)/shard_map/nid,njd->nij/dot_general | solution.py:93
  292.0 1.8 fusion.4
  293.9 4.3 %fusion.20 = f32[32,64,128]{2,1,0:T(8,128)} fusion(bf16[32,64,128]{2,1,0:T(8,128)(2,1)S(1)} %bitcast.97, bf16[32,64,64]{2,1,0:T(8,128)(2,1)} %fusion.26, bf16[32,64,256]{2,0,1:T(8,128)(2,1)} %copy-done.7, bf16[32,64,256]{2,0,1:T(8,128)(2,1)} %get-tuple-element.195, pred[64,64]{1,0:T(8,128)(4,1)S(1)} %iota_compare_fusion), kind=kOutput, calls=%fused_computation.32 | convolution fusion | flops 100794368 | bytes 3936256 | tf_op jit(solution)/shard_map/ucy,uyh->uch/dot_general | solution.py:104
  298.2 2.7 fusion.16
  301.7 26.1 %all_to_all.31 = bf16[16,1,64,128]{3,2,1,0:T(8,128)(2,1)S(1)} all-to-all(bf16[16,1,64,128]{3,2,1,0:T(8,128)(2,1)S(1)} %get-tuple-element.199), channel_id=1, replica_groups=mesh['sp'=16,'dp_0'=8,'dp_1'=4,'dp_2'=2] {'sp'}, dimensions={0} | all-to-all | bytes 524288 | tf_op jit(solution)/shard_map/all_to_all | solution.py:73
  327.7 6.0 %all-to-all-start.2 = ((bf16[16,1,64,128]{3,2,1,0:T(8,128)(2,1)}), bf16[16,1,64,128]{3,2,1,0:T(8,128)(2,1)S(1)}, u32[]{:S(2)}, u32[]{:S(2)}) async-start(bf16[16,1,64,128]{3,2,1,0:T(8,128)(2,1)} %get-tuple-element.198), calls=%async_computation.2 | async-start | bytes 524288 | tf_op jit(solution)/shard_map/all_to_all | solution.py:73
  334.0 18.2 %all-to-all-done.2 = bf16[16,1,64,128]{3,2,1,0:T(8,128)(2,1)S(1)} async-done(((bf16[16,1,64,128]{3,2,1,0:T(8,128)(2,1)}), bf16[16,1,64,128]{3,2,1,0:T(8,128)(2,1)S(1)}, u32[]{:S(2)}, u32[]{:S(2)}) %all-to-all-start.2) | async-done | bytes 262176 | tf_op jit(solution)/shard_map/all_to_all | solution.py:73
  (212 shorter events, 63.4 us)
Async XLA Ops:
  6.5 17.1 %copy-start = (bf16[1,128,2048]{2,1,0:T(8,128)(2,1)S(1)}, bf16[1,128,2048]{2,1,0:T(8,128)(2,1)}, u32[]{:S(2)}) copy-start(bf16[1,128,2048]{2,1,0:T(8,128)(2,1)} %param.13) | copy-start | bytes 1572868
  6.5 17.1 %copy-start.9 = (bf16[2048,16]{0,1:T(8,128)(2,1)S(1)}, bf16[2048,16]{0,1:T(8,128)(2,1)}, u32[]{:S(2)}) copy-start(bf16[2048,16]{0,1:T(8,128)(2,1)} %param.17) | copy-start | bytes 196612
  6.5 17.3 %copy-start.11 = (bf16[1,128]{1,0:T(2,128)(2,1)S(1)}, bf16[1,128]{1,0:T(2,128)(2,1)}, u32[]{:S(2)}) copy-start(bf16[1,128]{1,0:T(2,128)(2,1)} %param.20) | copy-start | bytes 772
  6.5 68.3 %all-gather.6.cloned.1.call-start = ((), (), s32[]{:S(2)}) async-start(), calls=%async_computation.4 | async-start | bytes 2359296 | tf_op jit(solution)/shard_map/all_gather | solution.py:30
  25.4 90.6 %all-to-all-start = ((bf16[16,128,401]{1,2,0:T(8,128)(2,1)}), bf16[16,128,401]{1,2,0:T(8,128)(2,1)S(1)}, u32[]{:S(2)}, u32[]{:S(2)}) async-start(bf16[16,128,401]{1,2,0:T(8,128)(2,1)} %pad_maximum_fusion), calls=%async_computation | async-start | bytes 3342336 | tf_op jit(solution)/shard_map/all_to_all | solution.py:49
  44.3 60.1 %all-gather.8.cloned.1.call-start = ((), (), s32[]{:S(2)}) async-start(), calls=%async_computation.5 | async-start | bytes 6291456 | tf_op jit(solution)/shard_map/all_gather | solution.py:30
  116.0 11.6 %copy-start.6 = (bf16[16,128,401]{1,2,0:T(8,128)(2,1)}, bf16[16,128,401]{1,2,0:T(8,128)(2,1)S(1)}, u32[]{:S(2)}) copy-start(bf16[16,128,401]{1,2,0:T(8,128)(2,1)S(1)} %all-to-all-done) | copy-start | bytes 4927492
  117.3 60.5 %all-to-all-start.1 = ((bf16[16,128,256]{2,1,0:T(8,128)(2,1)}), bf16[16,128,256]{2,1,0:T(8,128)(2,1)}, u32[]{:S(2)}, u32[]{:S(2)}) async-start(bf16[16,128,256]{2,1,0:T(8,128)(2,1)} %bitcast.16), calls=%async_computation.1 | async-start | bytes 2097152 | tf_op jit(solution)/shard_map/all_to_all | solution.py:166
  131.3 3.3 copy-start.1
  134.5 1.3 copy-start.3
  134.6 2.3 copy-start.2
  177.7 1.9 copy-start.4
  186.5 2.9 copy-start.7
  288.3 3.7 %copy-start.8 = (bf16[32,64,256]{2,0,1:T(8,128)(2,1)S(1)}, bf16[32,64,256]{2,0,1:T(8,128)(2,1)}, u32[]{:S(2)}) copy-start(bf16[32,64,256]{2,0,1:T(8,128)(2,1)} %get-tuple-element.195) | copy-start | bytes 3145732
  293.9 4.3 %copy-start.5 = (bf16[32,256,128]{2,1,0:T(8,128)(2,1)S(1)}, bf16[32,256,128]{2,1,0:T(8,128)(2,1)}, u32[]{:S(2)}) copy-start(bf16[32,256,128]{2,1,0:T(8,128)(2,1)} %get-tuple-element.135) | copy-start | bytes 6291460
  327.7 24.5 %all-to-all-start.2 = ((bf16[16,1,64,128]{3,2,1,0:T(8,128)(2,1)}), bf16[16,1,64,128]{3,2,1,0:T(8,128)(2,1)S(1)}, u32[]{:S(2)}, u32[]{:S(2)}) async-start(bf16[16,1,64,128]{3,2,1,0:T(8,128)(2,1)} %get-tuple-element.198), calls=%async_computation.2 | async-start | bytes 524288 | tf_op jit(solution)/shard_map/all_to_all | solution.py:73
  334.0 19.2 %copy-start.10 = (f32[2048]{0:T(1024)S(1)}, f32[2048]{0:T(1024)}, u32[]{:S(2)}) copy-start(f32[2048]{0:T(1024)} %param.21) | copy-start | bytes 24580
Sparse Core Ops, SparseCore 0:
  21.0 53.7 all-gather.5
  77.5 26.8 all-gather.7
where the time goes:
time: 363 us; the launch traced here: 361 us
  waiting for transfers between devices  126 us (35%)
  other arithmetic  103 us (28%)
  blocking collectives  40.4 us (11%)
  starting transfers between devices  35.2 us (10%)
  matrix products  23.4 us (6%)
  local copies, waits for them, and re-layouts  17.2 us (5%)
  between operations  13.7 us (4%)
    all_gather x2, waiting for transfers between devices, gather_in_order(): parts = lax.all_gather(parts, axes[k])  60 us
    all_to_all x1, waiting for transfers between devices, body(): lax.all_to_all(per_item(keys, DK), 'sp', split_axis=0, concat_axis=1, til...  39.4 us
    add x32, other arithmetic, backward_step(): return (state_here + term, state_here)  32.7 us
    add x32, other arithmetic, forward_step(): return (rate[:, None] * carry_state + term, carry_state)  32.4 us
    all_to_all x1, blocking collectives, exchange_in_pieces(): lax.all_to_all(piece, axis, split_axis=0, concat_axis=0, tiled=True)  26.1 us
    dynamic_update_slice x64, other arithmetic, mechanism(): _, forward_scan_states = lax.scan(forward_step, empty, (rates, end_terms))  24.4 us
    all_to_all x1, starting transfers between devices, side_by_side(): lax.all_to_all(both, axis, split_axis=split_dim, concat_axis=concat_dim,...  18.9 us
    all_to_all x1, waiting for transfers between devices, exchange_in_pieces(): lax.all_to_all(piece, axis, split_axis=0, concat_axis=0, tiled=True)  18.2 us
  transfers between devices with their start and end apart: 5, of which 5 were waited for; matrix products, arithmetic and copies ran while one was open for 5% of the time, Pallas kernels for 0%

commit v1 on v0

v1 whole, which is shorter than its diff:
```python
import functools

import jax
import jax.numpy as jnp
from jax import lax
from jax.experimental import pallas as pl
from jax.experimental.pallas import tpu as pltpu
from jax.sharding import Mesh
from jax.sharding import PartitionSpec as P

HEADS = 4
DK = 256
DV = 512
BLOCK = 64
TOK = 128
KEY = 1024
VAL = 2048
DP = ("y", "x", "c")
MESH = pl.DeviceIdType.MESH

GROUPS = 4
ROWS = 32
LAG_NUM, LAG_DEN = 9, 2

decay_tau = 16.0
norm_eps = 1e-05
f32 = jnp.float32
bf16 = jnp.bfloat16
highest = lax.Precision.HIGHEST


def kernel(
    sizes,
    hid_in, q_in, v_in, kw_in, down, up, bias, shift, gain, out,
    hid, q, v, kw, w,
    e1, e2, e3, ends, qf, qb, qe, qF, qB, kf, kb, ke, rate, term, came, went, acc, low,
    in_sem, own_sem, y_send, y_recv, x_send, x_recv, f_send, f_recv, d_send, d_recv,
    s_send, s_recv,
):
    Z, Y, X, C = sizes
    z, y, x, c = (lax.axis_index(a) for a in ("sp", "y", "x", "c"))
    width = KEY // GROUPS
    chunks = KEY // ROWS
    xr, xl, xo = lax.rem(x + 1, X), lax.rem(x + X - 1, X), lax.rem(x + 2, X)
    half = Y // 2

    barrier = pltpu.get_barrier_semaphore()
    peers = [{"y": lax.rem(y + k, Y)} for k in range(1, Y)]
    peers += [{"x": xr}, {"x": xl}, {"c": 1 - c}]
    peers += [{"sp": lax.rem(z + 1, Z)}, {"sp": lax.rem(z + Z - 1, Z)}]
    for peer in peers:
        pl.semaphore_signal(barrier, inc=1, device_id=peer, device_id_type=MESH)

    loads = [
        pltpu.make_async_copy(kw_in, kw, in_sem.at[0]),
        pltpu.make_async_copy(hid_in.at[0], hid, in_sem.at[1]),
        pltpu.make_async_copy(q_in.at[0], q, in_sem.at[2]),
        pltpu.make_async_copy(v_in.at[0], v, in_sem.at[3]),
    ]
    for load in loads:
        load.start()
    owns = [
        pltpu.make_async_copy(kw_in.at[:, pl.ds(g * width, width)], w.at[g, y, x, c], own_sem.at[g])
        for g in range(GROUPS)
    ]
    for own in owns:
        own.start()
    loads[0].wait()
    pl.semaphore_wait(barrier, len(peers))

    def send(src, dst, s, r, peer):
        pltpu.make_async_remote_copy(
            src_ref=src, dst_ref=dst, send_sem=s, recv_sem=r, device_id=peer, device_id_type=MESH
        ).start()

    def wait(ref, sem):
        pltpu.make_async_copy(ref, ref, sem).wait()

    for g in range(GROUPS):
        for k in range(1, Y):
            send(
                kw.at[:, pl.ds(g * width, width)], w.at[g, y, x, c], y_send, y_recv.at[g],
                {"y": lax.rem(y + k, Y)},
            )

    @pl.when(z == 0)
    def _():
        came[0] = jnp.zeros((KEY, DV), bf16)

    @pl.when(z == Z - 1)
    def _():
        came[1] = jnp.zeros((KEY, DV), bf16)

    loads[1].wait()
    low[...] = jnp.dot(hid[...], down[...], preferred_element_type=f32).astype(bf16).astype(f32)
    loads[2].wait()

    row = lax.broadcasted_iota(jnp.int32, (TOK, TOK), 0)
    col = lax.broadcasted_iota(jnp.int32, (TOK, TOK), 1)
    same = (row < BLOCK) == (col < BLOCK)
    upto = jnp.where(same & (row >= col), 1.0, 0.0).astype(f32)
    moved = jnp.transpose(jnp.broadcast_to(shift[...].astype(f32), (TOK, TOK)))
    first = row < BLOCK

    def spread(top, bottom):
        return jnp.where(first, jnp.broadcast_to(top, (TOK, TOK)), jnp.broadcast_to(bottom, (TOK, TOK)))

    @pl.loop(0, KEY // 128)
    def _(j):
        at = pl.ds(pl.multiple_of(j * 128, 128), 128)
        pre = jnp.dot(low[...], up[:, at], precision=highest, preferred_element_type=f32)
        pre = pre + bias[:, at] + moved
        log_decay = (jnp.minimum(pre, 0.0) - jnp.log1p(jnp.exp(-jnp.abs(pre)))) / decay_tau
        inclusive = jnp.dot(upto, log_decay, precision=highest, preferred_element_type=f32)
        exclusive = inclusive - log_decay
        total0, total1 = inclusive[BLOCK - 1 : BLOCK, :], inclusive[TOK - 1 : TOK, :]
        total = spread(total0, total1)
        one = jnp.ones((1, TOK), f32)
        end0, end1 = jnp.exp(total0), jnp.exp(total1)
        ends[0:1, at] = end0
        ends[1:2, at] = end1
        e1[:, at] = jnp.exp(-inclusive)
        e2[:, at] = jnp.exp(exclusive)
        e3[:, at] = jnp.exp(total - inclusive)
        scaled = q[:, at].astype(f32) * DK ** (-0.5)
        forward = scaled * jnp.exp(inclusive)
        reverse = scaled * jnp.exp(total - exclusive)
        qf[:, at] = forward.astype(bf16)
        qb[:, at] = (scaled * jnp.exp(-exclusive)).astype(bf16)
        qe[:, at] = reverse.astype(bf16)
        qF[:, at] = (forward * spread(one, end0)).astype(bf16)
        qB[:, at] = (reverse * spread(end1, one)).astype(bf16)
        rate[at, :] = jnp.transpose(jnp.broadcast_to(end0 * end1, (TOK, TOK)))

    loads[3].wait()

    def after_y(g):
        owns[g].wait()
        wait(w.at[g, pl.ds(0, Y - 1), x, c], y_recv.at[g])
        part = w.at[g, :, x, c]
        send(part, part, x_send.at[0], x_recv.at[0, g], {"x": xr})
        send(part, part, x_send.at[1], x_recv.at[1, g], {"x": xl})
        send(part, part, d_send, d_recv.at[g], {"c": 1 - c})

    def after_x(g):
        for k, (source, target, at) in enumerate(((xl, xr, 0), (xr, xl, half))):
            part = w.at[g, :, source, c]
            wait(part, x_recv.at[k, g])
            piece = w.at[g, pl.ds(at, half), source, c]
            send(piece, piece, f_send.at[k], f_recv.at[k, g], {"x": target})
            send(part, part, d_send, d_recv.at[g], {"c": 1 - c})

    def after_f(g):
        for k, at in enumerate((0, half)):
            wait(w.at[g, pl.ds(at, half), xo, c], f_recv.at[k, g])
        part = w.at[g, :, xo, c]
        send(part, part, d_send, d_recv.at[g], {"c": 1 - c})

    def project(g):
        wait(w.at[g, :, :, 1 - c], d_recv.at[g])
        at = pl.ds(g * width, width)
        head = g * width // DK
        wide = (TOK, width)
        weight = w[g].reshape(Y * X * C * kw.shape[0], width)
        keys = jnp.dot(hid[...], weight, preferred_element_type=f32).astype(bf16).astype(f32)
        rows = lax.broadcasted_iota(jnp.int32, wide, 0) < BLOCK
        end0 = jnp.where(rows, 1.0, jnp.broadcast_to(ends[0:1, at], wide))
        end1 = jnp.where(rows, jnp.broadcast_to(ends[1:2, at], wide), 1.0)
        key_bwd = keys * e2[:, at]
        key_end = keys * e3[:, at]
        kf[:, at] = (keys * e1[:, at]).astype(bf16)
        kb[:, at] = key_bwd.astype(bf16)
        ke[:, at] = key_end.astype(bf16)
        value = v[:, pl.ds(head * DV, DV)]
        over_tokens = (((0,), (0,)), ((), ()))
        term[0, at, :] = lax.dot_general(
            (key_end * end1).astype(bf16), value, over_tokens, preferred_element_type=f32
        )
        term[1, at, :] = lax.dot_general(
            (key_bwd * end0).astype(bf16), value, over_tokens, preferred_element_type=f32
        )

    for s in range(GROUPS + 3):
        for late, stage in enumerate((after_y, after_x, after_f, project)):
            if 0 <= s - late < GROUPS:
                stage(s - late)

    def within(h):
        at = pl.ds(pl.multiple_of(h * DK, DK), DK)
        to = pl.ds(pl.multiple_of(h * DV, DV), DV)
        over_channels = (((1,), (1,)), ((), ()))

        def scores(a, b):
            return lax.dot_general(a[:, at], b[:, at], over_channels, preferred_element_type=f32)

        near = jnp.where(row >= col, scores(qf, kf), scores(qb, kb))
        far = jnp.where(row >= col, scores(qf, ke), scores(qe, kb))
        both = jnp.where(same, near, far).astype(bf16)
        acc[:, to] = jnp.dot(both, v[:, to], preferred_element_type=f32)

    def step(d, n):
        at = pl.ds(pl.multiple_of(n * ROWS, ROWS), ROWS)
        has_prev = jnp.where(d == 0, z > 0, z < Z - 1)
        has_next = jnp.where(d == 0, z < Z - 1, z > 0)
        target = jnp.where(d == 0, lax.rem(z + 1, Z), lax.rem(z + Z - 1, Z))

        @pl.when(has_prev)
        def _():
            wait(came.at[d, at, :], s_recv.at[d, n])

        @pl.when(has_next)
        def _():
            for k in range(DV // 128):
                lanes = pl.ds(k * 128, 128)
                went[d, at, lanes] = (
                    came[d, at, lanes].astype(f32) * rate[at, :] + term[d, at, lanes]
                ).astype(bf16)
            send(went.at[d, at, :], came.at[d, at, :], s_send.at[d], s_recv.at[d, n], {"sp": target})

    early = jnp.where(2 * z < Z, 0, 1)
    apart = jnp.where(2 * z < Z, Z - 1 - 2 * z, 2 * z - (Z - 1))
    lag = jnp.minimum(apart * LAG_NUM // LAG_DEN, chunks)
    at_end = (z == 0) | (z == Z - 1)
    start = jnp.where(at_end, chunks, 0)

    @pl.loop(0, chunks + jnp.maximum(lag, HEADS))
    def _(m):
        @pl.when((m >= start) & (m < start + HEADS))
        def _():
            within(m - start)

        @pl.when(m < chunks)
        def _():
            step(early, m)

        @pl.when((m >= lag) & (m - lag < chunks))
        def _():
            step(1 - early, m - lag)

    @pl.loop(0, HEADS)
    def _(h):
        at = pl.ds(pl.multiple_of(h * DK, DK), DK)
        to = pl.ds(pl.multiple_of(h * DV, DV), DV)
        mixed = acc[:, to] + jnp.dot(qF[:, at], came[0, at, :], preferred_element_type=f32)
        mixed = mixed + jnp.dot(qB[:, at], came[1, at, :], preferred_element_type=f32)
        mixed = mixed.astype(bf16).astype(f32)
        mean = jnp.mean(mixed * mixed, axis=-1, keepdims=True)
        out[0, :, to] = (mixed * lax.rsqrt(mean + norm_eps) * gain[:, to]).astype(bf16)

    wait(w.at[:, pl.ds(0, Y - 1), 0, 0], y_send)
    for k in range(2):
        wait(w.at[:, :, 0, 0], x_send.at[k])
        wait(w.at[:, pl.ds(0, half), 0, 0], f_send.at[k])
    wait(w.at[:, :, :, 0], d_send)

    @pl.when(z < Z - 1)
    def _():
        wait(went.at[0], s_send.at[0])

    @pl.when(z > 0)
    def _():
        wait(went.at[1], s_send.at[1])


def body(sizes, hidden, queries, values, key_weight, decay_down, decay_up, decay_bias, span_shift, norm_gain):
    Z, Y, X, C = sizes
    D = hidden.shape[-1]
    chunks = KEY // ROWS
    hbm = pl.BlockSpec(memory_space=pl.ANY)
    vmem = pl.BlockSpec(memory_space=pltpu.VMEM)
    dma = pltpu.SemaphoreType.DMA
    tokens_by_key = lambda t: pltpu.VMEM((TOK, KEY), t)
    return pl.pallas_call(
        functools.partial(kernel, sizes),
        out_shape=jax.ShapeDtypeStruct((1, TOK, VAL), bf16),
        in_specs=[hbm] * 4 + [vmem] * 5,
        out_specs=vmem,
        scratch_shapes=[
            pltpu.VMEM((TOK, D), bf16),
            pltpu.VMEM((TOK, KEY), bf16),
            pltpu.VMEM((TOK, VAL), bf16),
            pltpu.VMEM(key_weight.shape, bf16),
            pltpu.VMEM((GROUPS, Y, X, C, key_weight.shape[0], KEY // GROUPS), bf16),
            tokens_by_key(f32), tokens_by_key(f32), tokens_by_key(f32),
            pltpu.VMEM((2, KEY), f32),
        ] + [tokens_by_key(bf16)] * 8 + [
            pltpu.VMEM((KEY, 128), f32),
            pltpu.VMEM((2, KEY, DV), f32),
            pltpu.VMEM((2, KEY, DV), bf16),
            pltpu.VMEM((2, KEY, DV), bf16),
            pltpu.VMEM((TOK, VAL), f32),
            pltpu.VMEM((TOK, 16), f32),
            dma((4,)), dma((GROUPS,)), dma, dma((GROUPS,)), dma((2,)), dma((2, GROUPS)),
            dma((2,)), dma((2, GROUPS)), dma, dma((GROUPS,)), dma((2,)), dma((2, chunks)),
        ],
        compiler_params=pltpu.CompilerParams(collective_id=0, has_side_effects=True),
    )(
        hidden, queries, values, key_weight, decay_down, decay_up,
        decay_bias.reshape(1, KEY), span_shift, norm_gain.reshape(1, VAL),
    )


def solution(mesh):
    split = Mesh(mesh.devices.reshape(mesh.shape["sp"], 8, 4, 2), ("sp", "y", "x", "c"))
    return build(split)


def build(split):
    placed = (
        P(DP, "sp", None),
        P(DP, "sp", None),
        P(DP, "sp", None),
        P(DP, None),
        P(),
        P(),
        P(),
        P(DP, "sp"),
        P(),
    )
    sizes = tuple(split.shape[a] for a in ("sp", "y", "x", "c"))
    return jax.shard_map(
        functools.partial(body, sizes),
        mesh=split, in_specs=placed, out_specs=P(DP, "sp", None), check_vma=False,
    )
```

time: 363 us -> 127 us (0.35)
  waiting for transfers between devices: 126 us -> 0 us
  Pallas kernels: 0 us -> 123 us
  other arithmetic: 103 us -> 0 us
  blocking collectives: 40.4 us -> 0 us
  starting transfers between devices: 35.2 us -> 0 us
  matrix products: 23.4 us -> 0 us
  between operations: 13.7 us -> 0.01 us
  local copies, waits for them, and re-layouts: 17.2 us -> 3.72 us
    pallas_call x0 -> x1, Pallas kernels: none -> 123 us  [body(): pl.pallas_call(functools.partial(kernel, sizes), out_shape=jax.ShapeDtype...]
    all_to_all x3 -> x0, waiting for transfers between devices: 65.6 us -> none  [the longest x1 39.4 us: body(): lax.all_to_all(per_item(keys, DK), 'sp', split_axis=0, concat_axis=1, til...]
    add x64 -> x0, other arithmetic: 65.1 us -> none  [the longest x32 32.7 us: backward_step(): return (state_here + term, state_here)]
    all_gather x2 -> x0, waiting for transfers between devices: 60 us -> none  [gather_in_order(): parts = lax.all_gather(parts, axes[k])]
    all_to_all x3 -> x0, starting transfers between devices: 35.1 us -> none  [the longest x1 18.9 us: side_by_side(): lax.all_to_all(both, axis, split_axis=split_dim, concat_axis=concat_dim,...]
    all_to_all x1 -> x0, blocking collectives: 26.1 us -> none  [exchange_in_pieces(): lax.all_to_all(piece, axis, split_axis=0, concat_axis=0, tiled=True)]
    dynamic_update_slice x64 -> x0, other arithmetic: 24.4 us -> none  [mechanism(): _, forward_scan_states = lax.scan(forward_step, empty, (rates, end_terms))]
    dot_general x9 -> x0, matrix products: 23.4 us -> none  [the longest x1 4.31 us: mechanism(): jnp.einsum('ucy,uyh->uch', attention_scores, value_tensor3, preferred_ele...]
  transfers between devices with their start and end apart: 5 -> 0, of which waited for: 5 -> 0; matrix products, arithmetic and copies ran while one was open for 5% -> 0% of each run, Pallas kernels for 0% -> 0%
where the time goes in v1:
time: 127 us
  Pallas kernels  123 us (97%)
  local copies, waits for them, and re-layouts  3.72 us (3%)
    pallas_call x1, Pallas kernels, body(): pl.pallas_call(functools.partial(kernel, sizes), out_shape=jax.ShapeDtype...  123 us
    unnamed x2, local copies, waits for them, and re-layouts  3.72 us

profile of v1, /device:TPU:56, one launch (start us, length us, event | category | flops | bytes accessed | tf_op | source)
XLA Modules:
  0.0 126.8 jit_solution(10004709462399027302)
XLA Ops:
  0.0 1.8 %copy.10.down = bf16[2048,16]{1,0:T(8,128)(2,1)} copy(bf16[2048,16]{0,1:T(8,128)(2,1)} %param.13) | data formatting | bytes 131072 | tf_op args[4]
  1.8 123.0 %shard_map.91 = bf16[1,128,2048]{2,1,0:T(8,128)(2,1)} custom-call(bf16[1,128,2048]{2,1,0:T(8,128)(2,1)} %hid_in.1, bf16[1,128,1024]{2,1,0:T(8,128)(2,1)} %q_in.1, bf16[1,128,2048]{2,1,0:T(8,128)(2,1)} %v_in.1, bf16[32,1024]{1,0:T(8,128)(2,1)} %kw_in.1, bf16[2048,16]{1,0:T(8,128)(2,1)} %copy.10.down, f32[16,1024]{1,0:T(8,128)} %up.1, f32[1,1024]{1,0:T(1,128)} %bitcast.3, ...), custom_call_target="tpu_custom_call" | custom-call | tf_op jit(solution)/shard_map/pallas_call | solution.py:273
  124.9 1.9 %copy.12 = bf16[1,128,2048]{2,1,0:T(8,128)(2,1)} copy(bf16[1,128,2048]{2,1,0:T(8,128)(2,1)} %shard_map.91) | data formatting | bytes 1048576

commit v2 on v1

--- a/solution.py
+++ b/solution.py
@@ -19,8 +19,9 @@
 MESH = pl.DeviceIdType.MESH
 
 GROUPS = 4
-ROWS = 32
-LAG_NUM, LAG_DEN = 9, 2
+ROWS = 16
+LAG = 34
+PACE = 12
 
 decay_tau = 16.0
 norm_eps = 1e-05
@@ -35,7 +36,7 @@
     hid, q, v, kw, w,
     e1, e2, e3, ends, qf, qb, qe, qF, qB, kf, kb, ke, rate, term, came, went, acc, low,
     in_sem, own_sem, y_send, y_recv, x_send, x_recv, f_send, f_recv, d_send, d_recv,
-    s_send, s_recv,
+    s_send, s_recv, o_sem, res,
 ):
     Z, Y, X, C = sizes
     z, y, x, c = (lax.axis_index(a) for a in ("sp", "y", "x", "c"))
@@ -43,6 +44,7 @@
     chunks = KEY // ROWS
     xr, xl, xo = lax.rem(x + 1, X), lax.rem(x + X - 1, X), lax.rem(x + 2, X)
     half = Y // 2
+    over_channels = (((1,), (1,)), ((), ()))
 
     barrier = pltpu.get_barrier_semaphore()
     peers = [{"y": lax.rem(y + k, Y)} for k in range(1, Y)]
@@ -92,7 +94,11 @@
         came[1] = jnp.zeros((KEY, DV), bf16)
 
     loads[1].wait()
-    low[...] = jnp.dot(hid[...], down[...], preferred_element_type=f32).astype(bf16).astype(f32)
+    low[...] = (
+        lax.dot_general(hid[...], down[...], over_channels, preferred_element_type=f32)
+        .astype(bf16)
+        .astype(f32)
+    )
     loads[2].wait()
 
     row = lax.broadcasted_iota(jnp.int32, (TOK, TOK), 0)
@@ -180,16 +186,9 @@
             (key_bwd * end0).astype(bf16), value, over_tokens, preferred_element_type=f32
         )
 
-    for s in range(GROUPS + 3):
-        for late, stage in enumerate((after_y, after_x, after_f, project)):
-            if 0 <= s - late < GROUPS:
-                stage(s - late)
-
     def within(h):
         at = pl.ds(pl.multiple_of(h * DK, DK), DK)
         to = pl.ds(pl.multiple_of(h * DV, DV), DV)
-        over_channels = (((1,), (1,)), ((), ()))
-
         def scores(a, b):
             return lax.dot_general(a[:, at], b[:, at], over_channels, preferred_element_type=f32)
 
@@ -217,36 +216,65 @@
                 ).astype(bf16)
             send(went.at[d, at, :], came.at[d, at, :], s_send.at[d], s_recv.at[d, n], {"sp": target})
 
-    early = jnp.where(2 * z < Z, 0, 1)
-    apart = jnp.where(2 * z < Z, Z - 1 - 2 * z, 2 * z - (Z - 1))
-    lag = jnp.minimum(apart * LAG_NUM // LAG_DEN, chunks)
-    at_end = (z == 0) | (z == Z - 1)
-    start = jnp.where(at_end, chunks, 0)
-
-    @pl.loop(0, chunks + jnp.maximum(lag, HEADS))
-    def _(m):
-        @pl.when((m >= start) & (m < start + HEADS))
-        def _():
-            within(m - start)
-
-        @pl.when(m < chunks)
-        def _():
-            step(early, m)
-
-        @pl.when((m >= lag) & (m - lag < chunks))
-        def _():
-            step(1 - early, m - lag)
-
-    @pl.loop(0, HEADS)
-    def _(h):
+    def finish(h):
         at = pl.ds(pl.multiple_of(h * DK, DK), DK)
         to = pl.ds(pl.multiple_of(h * DV, DV), DV)
         mixed = acc[:, to] + jnp.dot(qF[:, at], came[0, at, :], preferred_element_type=f32)
         mixed = mixed + jnp.dot(qB[:, at], came[1, at, :], preferred_element_type=f32)
         mixed = mixed.astype(bf16).astype(f32)
         mean = jnp.mean(mixed * mixed, axis=-1, keepdims=True)
-        out[0, :, to] = (mixed * lax.rsqrt(mean + norm_eps) * gain[:, to]).astype(bf16)
-
+        res[:, to] = (mixed * lax.rsqrt(mean + norm_eps) * gain[:, to]).astype(bf16)
+        pltpu.make_async_copy(res.at[:, to], out.at[0, :, to], o_sem.at[h]).start()
+
+    early = jnp.where(2 * z < Z, 0, 1)
+    edge = jnp.minimum(z, Z - 1 - z)
+    per_head = DK // ROWS
+    lag = jnp.where(edge == 0, chunks, jnp.minimum((Z - 1 - 2 * edge) * LAG // 4, chunks))
+
+    def before(g):
+        part = chunks * g // GROUPS
+        return jnp.where(edge == 0, part, jnp.clip(PACE * g - edge * LAG // 4, 0, part))
+
+    start = jnp.where(edge == 0, chunks, before(GROUPS - 1))
+
+    def chain(lo, hi):
+        @pl.loop(lo, hi)
+        def _(m):
+            @pl.when((m >= start) & (m < start + HEADS))
+            def _():
+                within(m - start)
+
+            @pl.when(m < chunks)
+            def _():
+                step(early, m)
+
+            n = m - lag
+
+            @pl.when((n >= 0) & (n < chunks))
+            def _():
+                step(1 - early, n)
+
+                @pl.when(lax.rem(n, per_head) == per_head - 1)
+                def _():
+                    finish(n // per_head)
+
+    for s in range(GROUPS + 3):
+        if s >= 3:
+            g = s - 3
+            project(g)
+            if g < GROUPS - 1:
+                chain(before(g), before(g + 1))
+        if 0 <= s - 2 < GROUPS:
+            after_f(s - 2)
+        if 0 <= s - 1 < GROUPS:
+            after_x(s - 1)
+        if s < GROUPS:
+            after_y(s)
+    chain(before(GROUPS - 1), chunks + jnp.maximum(lag, HEADS))
+
+    for h in range(HEADS):
+        to = pl.ds(h * DV, DV)
+        pltpu.make_async_copy(res.at[:, to], out.at[0, :, to], o_sem.at[h]).wait()
     wait(w.at[:, pl.ds(0, Y - 1), 0, 0], y_send)
     for k in range(2):
         wait(w.at[:, :, 0, 0], x_send.at[k])
@@ -274,7 +302,7 @@
         functools.partial(kernel, sizes),
         out_shape=jax.ShapeDtypeStruct((1, TOK, VAL), bf16),
         in_specs=[hbm] * 4 + [vmem] * 5,
-        out_specs=vmem,
+        out_specs=hbm,
         scratch_shapes=[
             pltpu.VMEM((TOK, D), bf16),
             pltpu.VMEM((TOK, KEY), bf16),
@@ -292,10 +320,11 @@
             pltpu.VMEM((TOK, 16), f32),
             dma((4,)), dma((GROUPS,)), dma, dma((GROUPS,)), dma((2,)), dma((2, GROUPS)),
             dma((2,)), dma((2, GROUPS)), dma, dma((GROUPS,)), dma((2,)), dma((2, chunks)),
+            dma((HEADS,)), pltpu.VMEM((TOK, VAL), bf16),
         ],
         compiler_params=pltpu.CompilerParams(collective_id=0, has_side_effects=True),
     )(
-        hidden, queries, values, key_weight, decay_down, decay_up,
+        hidden, queries, values, key_weight, decay_down.T, decay_up,
         decay_bias.reshape(1, KEY), span_shift, norm_gain.reshape(1, VAL),
     )
 

time: 127 us -> 118 us (0.929)
  the two profiles are of different devices: /device:TPU:56 before, /device:TPU:2 now
where the time goes in v2:
time: 118 us
  Pallas kernels  116 us (98%)
  local copies, waits for them, and re-layouts  1.88 us (2%)
    pallas_call x1, Pallas kernels, body(): pl.pallas_call(functools.partial(kernel, sizes), out_shape=jax.ShapeDtype...  116 us

profile of v2, /device:TPU:2, one launch (start us, length us, event | category | flops | bytes accessed | tf_op | source)
XLA Modules:
  0.0 117.6 jit_solution(13128847509851069687)
XLA Ops:
  0.0 115.7 %shard_map.91 = bf16[1,128,2048]{2,1,0:T(8,128)(2,1)} custom-call(bf16[1,128,2048]{2,1,0:T(8,128)(2,1)} %hid_in.1, bf16[1,128,1024]{2,1,0:T(8,128)(2,1)} %q_in.1, bf16[1,128,2048]{2,1,0:T(8,128)(2,1)} %v_in.1, bf16[32,1024]{1,0:T(8,128)(2,1)} %kw_in.1, bf16[16,2048]{1,0:T(8,128)(2,1)} %bitcast.3, f32[16,1024]{1,0:T(8,128)} %up.1, f32[1,1024]{1,0:T(1,128)} %bitcast.5, ...), custom_call_target="tpu_custom_call" | custom-call | tf_op jit(solution)/shard_map/pallas_call | solution.py:301
  115.7 1.9 %copy.11 = bf16[1,128,2048]{2,1,0:T(8,128)(2,1)} copy(bf16[1,128,2048]{2,1,0:T(8,128)(2,1)} %shard_map.91) | data formatting | bytes 1048576

commit v3 on v2

--- a/solution.py
+++ b/solution.py
@@ -22,6 +22,7 @@
 ROWS = 16
 LAG = 34
 PACE = 12
+SKEW = -16
 
 decay_tau = 16.0
 norm_eps = 1e-05
@@ -226,23 +227,23 @@
         res[:, to] = (mixed * lax.rsqrt(mean + norm_eps) * gain[:, to]).astype(bf16)
         pltpu.make_async_copy(res.at[:, to], out.at[0, :, to], o_sem.at[h]).start()
 
-    early = jnp.where(2 * z < Z, 0, 1)
-    edge = jnp.minimum(z, Z - 1 - z)
+    ahead = (Z - 1 - 2 * z) * LAG + SKEW * 4
+    early = jnp.where(ahead >= 0, 0, 1)
+    edge = jnp.where(ahead >= 0, z, Z - 1 - z)
     per_head = DK // ROWS
-    lag = jnp.where(edge == 0, chunks, jnp.minimum((Z - 1 - 2 * edge) * LAG // 4, chunks))
+    lag = jnp.where(edge == 0, chunks, jnp.minimum(jnp.abs(ahead) // 4, chunks))
+    far = lag == chunks
 
     def before(g):
         part = chunks * g // GROUPS
         return jnp.where(edge == 0, part, jnp.clip(PACE * g - edge * LAG // 4, 0, part))
 
-    start = jnp.where(edge == 0, chunks, before(GROUPS - 1))
-
     def chain(lo, hi):
         @pl.loop(lo, hi)
         def _(m):
-            @pl.when((m >= start) & (m < start + HEADS))
+            @pl.when(far & (m >= chunks) & (m < chunks + HEADS))
             def _():
-                within(m - start)
+                within(m - chunks)
 
             @pl.when(m < chunks)
             def _():
@@ -254,7 +255,7 @@
             def _():
                 step(1 - early, n)
 
-                @pl.when(lax.rem(n, per_head) == per_head - 1)
+                @pl.when(far & (lax.rem(n, per_head) == per_head - 1))
                 def _():
                     finish(n // per_head)
 
@@ -264,13 +265,24 @@
             project(g)
             if g < GROUPS - 1:
                 chain(before(g), before(g + 1))
+
+            @pl.when(jnp.logical_not(far))
+            def _():
+                within(g)
+
         if 0 <= s - 2 < GROUPS:
             after_f(s - 2)
         if 0 <= s - 1 < GROUPS:
             after_x(s - 1)
         if s < GROUPS:
             after_y(s)
-    chain(before(GROUPS - 1), chunks + jnp.maximum(lag, HEADS))
+    chain(before(GROUPS - 1), chunks + lag)
+
+    @pl.when(jnp.logical_not(far))
+    def _():
+        @pl.loop(0, HEADS)
+        def _(h):
+            finish(h)
 
     for h in range(HEADS):
         to = pl.ds(h * DV, DV)

time: 118 us -> 116 us (0.983)
  the two profiles are of different devices: /device:TPU:2 before, /device:TPU:56 now
where the time goes in v3:
time: 116 us; the launch traced here: 114 us
  Pallas kernels  113 us (97%)
  local copies, waits for them, and re-layouts  1.88 us (2%)
    pallas_call x1, Pallas kernels, body(): pl.pallas_call(functools.partial(kernel, sizes), out_shape=jax.ShapeDtype...  113 us

profile of v3, /device:TPU:56, one launch (start us, length us, event | category | flops | bytes accessed | tf_op | source)
XLA Modules:
  0.0 114.5 jit_solution(14022714793501075967)
XLA Ops:
  0.0 112.6 %shard_map.91 = bf16[1,128,2048]{2,1,0:T(8,128)(2,1)} custom-call(bf16[1,128,2048]{2,1,0:T(8,128)(2,1)} %hid_in.1, bf16[1,128,1024]{2,1,0:T(8,128)(2,1)} %q_in.1, bf16[1,128,2048]{2,1,0:T(8,128)(2,1)} %v_in.1, bf16[32,1024]{1,0:T(8,128)(2,1)} %kw_in.1, bf16[16,2048]{1,0:T(8,128)(2,1)} %bitcast.3, f32[16,1024]{1,0:T(8,128)} %up.1, f32[1,1024]{1,0:T(1,128)} %bitcast.5, ...), custom_call_target="tpu_custom_call" | custom-call | tf_op jit(solution)/shard_map/pallas_call | solution.py:313
  112.6 1.9 %copy.11 = bf16[1,128,2048]{2,1,0:T(8,128)(2,1)} copy(bf16[1,128,2048]{2,1,0:T(8,128)(2,1)} %shard_map.91) | data formatting | bytes 1048576

commit v4 on v3

--- a/solution.py
+++ b/solution.py
@@ -22,7 +22,7 @@
 ROWS = 16
 LAG = 34
 PACE = 12
-SKEW = -16
+SKEW = 0
 
 decay_tau = 16.0
 norm_eps = 1e-05
@@ -50,9 +50,17 @@
     barrier = pltpu.get_barrier_semaphore()
     peers = [{"y": lax.rem(y + k, Y)} for k in range(1, Y)]
     peers += [{"x": xr}, {"x": xl}, {"c": 1 - c}]
-    peers += [{"sp": lax.rem(z + 1, Z)}, {"sp": lax.rem(z + Z - 1, Z)}]
     for peer in peers:
         pl.semaphore_signal(barrier, inc=1, device_id=peer, device_id_type=MESH)
+
+    @pl.when(z < Z - 1)
+    def _():
+        pl.semaphore_signal(barrier, inc=1, device_id={"sp": lax.rem(z + 1, Z)}, device_id_type=MESH)
+
+    @pl.when(z > 0)
+    def _():
+        pl.semaphore_signal(barrier, inc=1, device_id={"sp": lax.rem(z + Z - 1, Z)}, device_id_type=MESH)
+
 
     loads = [
         pltpu.make_async_copy(kw_in, kw, in_sem.at[0]),
@@ -69,7 +77,7 @@
     for own in owns:
         own.start()
     loads[0].wait()
-    pl.semaphore_wait(barrier, len(peers))
+    pl.semaphore_wait(barrier, len(peers) + jnp.where((z == 0) | (z == Z - 1), 1, 2))
 
     def send(src, dst, s, r, peer):
         pltpu.make_async_remote_copy(
@@ -80,7 +88,7 @@
         pltpu.make_async_copy(ref, ref, sem).wait()
 
     for g in range(GROUPS):
-        for k in range(1, Y):
+        for k in sorted(range(1, Y), key=lambda k: -min(k, Y - k)):
             send(
                 kw.at[:, pl.ds(g * width, width)], w.at[g, y, x, c], y_send, y_recv.at[g],
                 {"y": lax.rem(y + k, Y)},

time: 116 us -> 115 us (level); the launches traced: 114 us -> 115 us
  no operation moved by 1% of the time
where the time goes in v4:
time: 115 us
  Pallas kernels  113 us (98%)
  local copies, waits for them, and re-layouts  1.88 us (2%)
    pallas_call x1, Pallas kernels, body(): pl.pallas_call(functools.partial(kernel, sizes), out_shape=jax.ShapeDtype...  113 us

profile of v4, /device:TPU:56, one launch (start us, length us, event | category | flops | bytes accessed | tf_op | source)
XLA Modules:
  0.0 114.8 jit_solution(12821786817953234060)
XLA Ops:
  0.0 112.9 %shard_map.91 = bf16[1,128,2048]{2,1,0:T(8,128)(2,1)} custom-call(bf16[1,128,2048]{2,1,0:T(8,128)(2,1)} %hid_in.1, bf16[1,128,1024]{2,1,0:T(8,128)(2,1)} %q_in.1, bf16[1,128,2048]{2,1,0:T(8,128)(2,1)} %v_in.1, bf16[32,1024]{1,0:T(8,128)(2,1)} %kw_in.1, bf16[16,2048]{1,0:T(8,128)(2,1)} %bitcast.3, f32[16,1024]{1,0:T(8,128)} %up.1, f32[1,1024]{1,0:T(1,128)} %bitcast.5, ...), custom_call_target="tpu_custom_call" | custom-call | tf_op jit(solution)/shard_map/pallas_call | solution.py:321
  112.9 1.9 %copy.11 = bf16[1,128,2048]{2,1,0:T(8,128)(2,1)} copy(bf16[1,128,2048]{2,1,0:T(8,128)(2,1)} %shard_map.91) | data formatting | bytes 1048576
